TPU v7x, 32 devices: a whole 2x2x4 slice. The times are simulated.
32 devices in a mesh: kv: 8 (over z, y), tp: 4 (over x, core).
Axes of the slice: x: 2, y: 2, z: 4, core: 2. Of those that a mesh axis runs over, the one named last changes fastest.
Arguments:
- tokens: bfloat16 [160, 4096], P(None, 'kv'), may hold values from -40 to 40
- input_norm_gain: float32 [4096], P('kv'), may hold values from 0.1 to 1.9
- input_matrix: bfloat16 [4096, 4096], P('kv', 'tp'), may hold values from -0.09375 to 0.09375
- gate_matrix: bfloat16 [4096, 4096], P('kv', 'tp'), may hold values from -0.09375 to 0.09375
- write_matrix: bfloat16 [4096, 1024], P('kv', 'tp'), may hold values from -0.09375 to 0.09375
- read_matrix: bfloat16 [4096, 1024], P('kv', 'tp'), may hold values from -0.09375 to 0.09375
- step_matrix: bfloat16 [4096, 64], replicated, may hold values from -0.09375 to 0.09375
- input_kernel: float32 [4, 4096], P(None, 'tp'), may hold values from -3 to 3
- write_kernel: float32 [4, 1024], P(None, 'tp'), may hold values from -3 to 3
- read_kernel: float32 [4, 1024], P(None, 'tp'), may hold values from -3 to 3
- step_size_bias: float32 [64], P('tp'), may hold values from -6 to 1
- head_decay_logs: float32 [64], P('tp'), may hold values from 0 to 2.77
- bypass_scale: float32 [64], P('tp'), may hold values from 0.5 to 1.5
- extra_decay_logs: float32 [160, 64], P('kv', 'tp'), may hold values from -0.7 to 0, as said below
- output_norm_gain: float32 [4096], P('tp'), may hold values from 0.1 to 1.9
- output_matrix: bfloat16 [4096, 4096], P('tp', 'kv'), may hold values from -0.09375 to 0.09375
- cached_state_history: float32 [32, 6, 64, 64, 128], P('kv', None, 'tp'), may hold values from -2 to 2
- cached_input_rows: bfloat16 [32, 8, 4096], P('kv', None, 'tp'), may hold values from -6 to 6
- cached_write_rows: bfloat16 [32, 8, 1024], P('kv', None, 'tp'), may hold values from -6 to 6
- cached_read_rows: bfloat16 [32, 8, 1024], P('kv', None, 'tp'), may hold values from -6 to 6
- accepted: int32 [32], P('kv'), may hold values from 0 to 5
Outputs:
- mixer_out: bfloat16 [160, 4096], P('tp', 'kv')
- next_states: float32 [32, 6, 64, 64, 128], P('kv', None, 'tp')
- next_input: bfloat16 [32, 8, 4096], P('kv', None, 'tp')
- next_write: bfloat16 [32, 8, 1024], P('kv', None, 'tp')
- next_read: bfloat16 [32, 8, 1024], P('kv', None, 'tp')
Inputs may be any that keep to these rules, and one draw needn't show every extreme that they name: `extra_decay_logs`: zero at most tokens and heads.
All inputs are finite; a program needn't handle non-finite values.
Results may differ from a plain program's by a relative error of at most 0.03.
Values may be sent and summed in bfloat16 or wider, within the bound.
A program may use at most 64 MiB of HBM per device.

v0:
```python
import jax
import jax.numpy as jnp
from jax import lax
from jax.sharding import PartitionSpec as P

D = 4096
HEAD_TOTAL = 64
P_SIZE = 64
N = 128
G = 8
TAPS = 4
DRAFT_TOKENS = 5


epsilon = 1e-05


def convolve(window, taps):
    total = jnp.zeros((window.shape[0], DRAFT_TOKENS, window.shape[2]), jnp.float32)
    for tap_index in range(TAPS):
        total = total + taps[tap_index] * window[:, tap_index : tap_index + DRAFT_TOKENS].astype(
            jnp.float32
        )
    return jax.nn.silu(total)


def per_device(
    tokens,
    input_norm_gain,
    input_matrix,
    gate_matrix,
    write_matrix,
    read_matrix,
    step_matrix,
    input_kernel,
    write_kernel,
    read_kernel,
    step_size_bias,
    head_decay_logs,
    bypass_scale,
    extra_decay_logs,
    output_norm_gain,
    output_matrix,
    cached_state_history,
    cached_input_rows,
    cached_write_rows,
    cached_read_rows,
    accepted,
):
    kv_count = lax.axis_size("kv")
    own_rows = tokens.shape[0] // kv_count
    local_sequences = own_rows // DRAFT_TOKENS
    local_width = tokens.shape[1]
    local_heads = step_size_bias.shape[0]
    groups_here = write_matrix.shape[1] // N
    input_width = input_matrix.shape[1]
    state_width = write_matrix.shape[1]
    wide_rows = tokens.astype(jnp.float32)
    scaled = (wide_rows * input_norm_gain).astype(jnp.bfloat16)
    weights = (input_matrix, gate_matrix, write_matrix, read_matrix)
    squares = jnp.sum(wide_rows * wide_rows, axis=1)
    step_block = lax.dynamic_slice(
        step_matrix,
        (lax.axis_index("kv") * local_width, lax.axis_index("tp") * local_heads),
        (local_width, local_heads),
    )
    step_term = jnp.dot(scaled, step_block, preferred_element_type=jnp.float32)
    joined = lax.psum_scatter(
        jnp.concatenate(
            [jnp.dot(scaled, weight, preferred_element_type=jnp.float32) for weight in weights],
            axis=1,
        ).astype(jnp.bfloat16),
        "kv",
        scatter_dimension=0,
        tiled=True,
    ).astype(jnp.float32)
    step_raw = lax.psum_scatter(
        step_term.astype(jnp.bfloat16), "kv", scatter_dimension=0, tiled=True
    ).astype(jnp.float32)
    square_sums = lax.psum_scatter(
        squares.astype(jnp.bfloat16), "kv", scatter_dimension=0, tiled=True
    ).astype(jnp.float32)
    inverse = lax.rsqrt(square_sums / D + epsilon)[:, None]
    joined = (joined * inverse).astype(jnp.bfloat16)
    fresh_input = joined[:, :input_width]
    fresh_gate = joined[:, input_width : 2 * input_width]
    fresh_write = joined[:, 2 * input_width : 2 * input_width + state_width]
    fresh_read = joined[:, 2 * input_width + state_width :]
    step_raw = step_raw * inverse
    row_picks = (
        jnp.arange(DRAFT_TOKENS + TAPS - 1, dtype=jnp.int32)[None, None, :]
        == accepted[:, None, None] + jnp.arange(TAPS - 1, dtype=jnp.int32)[None, :, None]
    ).astype(jnp.bfloat16)

    def make_window(saved, fresh):
        taken_rows = jnp.einsum(
            "srj,sjc->src", row_picks, saved, preferred_element_type=jnp.float32
        ).astype(jnp.bfloat16)
        return jnp.concatenate(
            [taken_rows, fresh.reshape(local_sequences, DRAFT_TOKENS, -1)], axis=1
        )

    next_input = make_window(cached_input_rows, fresh_input)
    next_write = make_window(cached_write_rows, fresh_write)
    next_read = make_window(cached_read_rows, fresh_read)
    conv_input = convolve(next_input, input_kernel).reshape(
        local_sequences, DRAFT_TOKENS, local_heads, P_SIZE
    )
    conv_write = jnp.repeat(
        convolve(next_write, write_kernel).reshape(local_sequences, DRAFT_TOKENS, groups_here, N),
        HEAD_TOTAL // G,
        axis=2,
    )
    conv_read = jnp.repeat(
        convolve(next_read, read_kernel).reshape(local_sequences, DRAFT_TOKENS, groups_here, N),
        HEAD_TOTAL // G,
        axis=2,
    )
    step_sizes = jax.nn.softplus(
        step_raw.reshape(local_sequences, DRAFT_TOKENS, local_heads) + step_size_bias
    )
    retain_logs = -step_sizes * jnp.exp(head_decay_logs) + extra_decay_logs.reshape(
        local_sequences, DRAFT_TOKENS, local_heads
    )
    chosen = jnp.arange(DRAFT_TOKENS + 1, dtype=jnp.int32)[None, :] == accepted[:, None]
    carried = jnp.sum(jnp.where(chosen[:, :, None, None, None], cached_state_history, 0.0), axis=1)
    states = [carried]
    outputs = []
    for position in range(DRAFT_TOKENS):
        written = (step_sizes[:, position, :, None] * conv_input[:, position])[:, :, :, None]
        carried = (
            jnp.exp(retain_logs[:, position])[:, :, None, None] * carried
            + written * conv_write[:, position][:, :, None, :]
        )
        states.append(carried)
        outputs.append(
            jnp.sum(carried * conv_read[:, position][:, :, None, :], axis=-1)
            + bypass_scale[:, None] * conv_input[:, position]
        )
    head_out = jnp.stack(outputs, axis=1).reshape(own_rows, input_width)
    gated = (head_out * jax.nn.silu(fresh_gate.astype(jnp.float32))).reshape(
        own_rows, groups_here, -1
    )
    gated = gated * lax.rsqrt(jnp.mean(gated * gated, axis=-1, keepdims=True) + epsilon)
    normed = (gated.reshape(own_rows, input_width) * output_norm_gain).astype(jnp.bfloat16)
    partial_value = jnp.dot(
        lax.all_gather(normed, "kv", axis=0, tiled=True),
        output_matrix,
        preferred_element_type=jnp.float32,
    )
    mixer_out = lax.psum_scatter(
        partial_value.astype(jnp.bfloat16), "tp", scatter_dimension=0, tiled=True
    )
    next_states = jnp.stack(states, axis=1)
    return (mixer_out, next_states, next_input, next_write, next_read)


def solution(mesh):
    return jax.shard_map(
        per_device,
        mesh=mesh,
        in_specs=(
            P(None, "kv"),
            P("kv"),
            P("kv", "tp"),
            P("kv", "tp"),
            P("kv", "tp"),
            P("kv", "tp"),
            P(),
            P(None, "tp"),
            P(None, "tp"),
            P(None, "tp"),
            P("tp"),
            P("tp"),
            P("tp"),
            P("kv", "tp"),
            P("tp"),
            P("tp", "kv"),
            P("kv", None, "tp", None, None),
            P("kv", None, "tp"),
            P("kv", None, "tp"),
            P("kv", None, "tp"),
            P("kv"),
        ),
        out_specs=(
            P("tp", "kv"),
            P("kv", None, "tp", None, None),
            P("kv", None, "tp"),
            P("kv", None, "tp"),
            P("kv", None, "tp"),
        ),
        check_vma=False,
    )
```

profile of v0, /device:TPU:0, one launch (start us, length us, event | category | flops | bytes accessed | tf_op | source)
XLA Modules:
  0.0 172.6 jit_solution(17806072741339071295)
XLA Ops:
  7.3 1.4 convolution_convert_fusion.4
  8.7 1.3 convolution_convert_fusion.3
  9.9 1.3 convolution_convert_fusion.1
  11.3 0.3 convolution_convert_fusion
  11.7 31.4 %fusion = bf16[24,2560]{1,0:T(8,128)(2,1)S(1)} fusion(bf16[160,2560]{1,0:T(8,128)(2,1)S(1)} %pad_maximum_fusion), kind=kCustom, calls=%all-reduce-scatter | all-reduce-scatter fusion | flops 491521 | bytes 942592
  43.2 2.0 %collective-permute-start = (bf16[24,2560]{1,0:T(8,128)(2,1)S(1)}, bf16[24,2560]{1,0:T(8,128)(2,1)}, u32[]{:S(2)}, u32[]{:S(2)}) collective-permute-start(bf16[24,2560]{1,0:T(8,128)(2,1)S(1)} %fusion), channel_id=1, source_target_pairs={{0,4},{4,8},{8,12},{12,16},{16,20},{20,24},{24,28},{1,5},{5,9},{9,... | collective-permute-start | bytes 368648
  45.2 1.3 collective-permute-start.1
  46.5 0.1 fusion.6
  46.8 0.6 fusion.42
  47.4 0.6 fusion.44
  48.6 0.9 convolution_convert_fusion.8
  49.5 20.5 %all-reduce.4 = (bf16[160]{0:T(256)(128)(2,1)S(1)}, bf16[160,16]{0,1:T(8,128)(2,1)S(1)}) all-reduce(bf16[160]{0:T(256)(128)(2,1)S(1)} %fusion.6, bf16[160,16]{0,1:T(8,128)(2,1)S(1)} %convolution_convert_fusion.8), channel_id=3, replica_groups=mesh['kv'=8,'tp'=4] {'kv'}, use_global_device_ids=true, to_apply=%region_2.0.clone | all-reduce | flops 2720 | bytes 10880
  70.3 0.8 convolution_convert_fusion.6
  71.1 0.8 convolution_convert_fusion.7
  72.0 0.6 fusion.41
  72.6 0.8 convolution_convert_fusion.5
  73.4 6.5 %select_reduce_fusion = f32[4,16,64,128]{3,2,1,0:T(8,128)S(1)} fusion(f32[4,6,16,64,128]{4,3,2,1,0:T(8,128)} %param.37, pred[4,6]{1,0:T(4,128)(4,1)S(1)} %iota_compare_fusion.4), kind=kLoop, calls=%fused_computation | loop fusion | flops 5767168 | bytes 14680088 | tf_op jit(solution)/shard_map/reduce_sum | solution.py:126
  80.0 1.5 bitcast_dynamic-update-slice_fusion
  81.5 0.6 slice_exponential_fusion.2
  82.1 0.6 fusion.43
  83.4 0.6 copy-done.16
  84.0 2.0 %concatenate.17 = bf16[52,2560]{1,0:T(8,128)(2,1)S(1)} concatenate(bf16[4,2560]{1,0:T(4,128)(2,1)} %copy-done.16, bf16[24,2560]{1,0:T(8,128)(2,1)} %collective-permute-done, bf16[24,2560]{1,0:T(8,128)(2,1)S(1)} %fusion), dimensions={0} | concatenate | bytes 532480
  86.0 0.7 multiply_convert_fusion
  86.7 0.6 copy-done.3
  87.4 0.9 divide_multiply_fusion.1
  88.3 1.3 pad_maximum_fusion.2
  89.6 0.9 divide_multiply_fusion.2
  90.6 1.4 pad_maximum_fusion.1
  92.0 1.0 divide_multiply_fusion
  93.1 0.1 reshape.262
  93.3 0.8 bitcast_multiply_fusion.3
  94.2 2.8 %multiply_reduce_fusion.3 = (f32[4,16,64]{2,1,0:T(8,128)S(1)}, f32[4,16,64]{2,1,0:T(8,128)S(1)}) fusion(f32[4,16,128]{2,1,0:T(8,128)S(1)} %get-tuple-element.17, f32[4,16,128]{2,1,0:T(8,128)S(1)} %get-tuple-element.61, f32[4,16,64]{2,1,0:T(8,128)S(1)} %get-tuple-element.22, f32[4,16,128]{2,1,0:T(8,128)S(1)} %get-tuple-element.60, ...), kind=kLoop, calls=%fused_computation.13 | loop fusion | flops 5234688 | bytes 2294272 | tf_op jit(solution)/shard_map/reduce_sum | solution.py:137
  97.1 0.7 fusion.24
  97.9 5.8 %multiply_reduce_fusion = (f32[4,16,64]{2,1,0:T(8,128)S(1)}, f32[4,16,64]{2,1,0:T(8,128)S(1)}, f32[4,16,64]{2,1,0:T(8,128)S(1)}) fusion(f32[4,16,128]{2,1,0:T(8,128)S(1)} %get-tuple-element.15, f32[4,16,128]{2,1,0:T(8,128)S(1)} %get-tuple-element.63, f32[4,16,64]{2,1,0:T(8,128)S(1)} %get-tuple-element.20, f32[4,16]{1,0:T(4,128)S(1)} %bitcast.138, ...), kind=kLoop, calls=%fused_computation.8 | loop fusion | flops 10997760 | bytes 2491648 | tf_op jit(solution)/shard_map/reduce_sum | solution.py:137
  103.9 0.7 copy.50
  104.6 1.0 reshape.269
  105.6 1.5 fusion.38
  107.1 1.6 mul.795
  108.7 1.0 reduce_sum.94
  109.9 0.9 fusion.19
  110.7 33.0 %all-gather = bf16[8,20,1024]{2,1,0:T(8,128)(2,1)} all-gather(bf16[1,20,1024]{2,1,0:T(8,128)(2,1)S(1)} %fusion.19), channel_id=1, replica_groups=mesh['kv'=8,'tp'=4] {'kv'}, dimensions={0}, use_global_device_ids=true | all-gather | bytes 368640 | tf_op jit(solution)/shard_map/all_gather | solution.py:147
  143.7 1.8 %reshape.271 = bf16[160,1024]{1,0:T(8,128)(2,1)} reshape(bf16[8,20,1024]{2,1,0:T(8,128)(2,1)} %all-gather) | data formatting | bytes 655360
  145.5 2.4 %convolution_convert_fusion.2 = bf16[160,512]{1,0:T(8,128)(2,1)} fusion(bf16[160,1024]{1,0:T(8,128)(2,1)} %reshape.271, bf16[1024,512]{1,0:T(8,128)(2,1)} %param.36), kind=kOutput, calls=%fused_computation.22 | convolution fusion | flops 167854080 | bytes 1540096 | tf_op jit(solution)/shard_map/dot_general | solution.py:146
  147.9 1.8 %fusion.4 = f32[4,6,16,64,128]{4,3,2,1,0:T(8,128)} fusion(f32[4,6,16,64,128]{4,3,2,1,0:T(8,128)} %bitcast_dynamic-update-slice_fusion, f32[4,16,64,128]{3,2,1,0:T(8,128)S(1)} %select_reduce_fusion, f32[4,16,128]{2,1,0:T(8,128)S(1)} %get-tuple-element.60, f32[4,16,64]{2,1,0:T(8,128)S(1)} %get-tuple-element.23, f32[4,16]{1,0:T(4,128)S(1)} %bitcast.120), kind=kLoop, calls=%fused_computation.19 | loop fusion | flops 1572864 | bytes 4243712
  149.6 2.8 %fusion.2 = f32[4,6,16,64,128]{4,3,2,1,0:T(8,128)} fusion(f32[4,6,16,64,128]{4,3,2,1,0:T(8,128)} %fusion.4, f32[4,16,64,128]{3,2,1,0:T(8,128)S(1)} %select_reduce_fusion, f32[4,16,128]{2,1,0:T(8,128)S(1)} %get-tuple-element.61, f32[4,16,64]{2,1,0:T(8,128)S(1)} %get-tuple-element.22, f32[4,16]{1,0:T(4,128)S(1)} %bitcast.127, ...), kind=kLoop, calls=%fused_computation.17 | loop fusion | flops 3145728 | bytes 4293120
  152.4 3.3 %constant_dynamic-update-slice_fusion = f32[4,6,16,64,128]{4,3,2,1,0:T(8,128)} fusion(f32[4,6,16,64,128]{4,3,2,1,0:T(8,128)} %fusion.2, f32[4,16,128]{2,1,0:T(8,128)S(1)} %get-tuple-element.64, f32[4,16,64]{2,1,0:T(8,128)S(1)} %get-tuple-element.19, f32[4,16,128]{2,1,0:T(8,128)S(1)} %get-tuple-element.61, f32[4,16,64]{2,1,0:T(8,128)S(1)} %get-tuple-element.22, ...), kind=kLoop, calls=%fused_computation.82 | loop fusion | flops 4718592 | bytes 4342528
  155.7 4.8 %fusion.3 = f32[4,6,16,64,128]{4,3,2,1,0:T(8,128)} fusion(f32[4,6,16,64,128]{4,3,2,1,0:T(8,128)} %constant_dynamic-update-slice_fusion, f32[4,16,128]{2,1,0:T(8,128)S(1)} %get-tuple-element.62, f32[4,16,64]{2,1,0:T(8,128)S(1)} %copy-done.5, f32[4,16]{1,0:T(4,128)S(1)} %bitcast.136, f32[4,16,128]{2,1,0:T(8,128)S(1)} %get-tuple-element.64, ...), kind=kLoop, calls=%fused_computation.18 | loop fusion | flops 6291456 | bytes 4391936
  160.5 5.2 %add_dynamic-update-slice_fusion = f32[4,6,16,64,128]{4,3,2,1,0:T(8,128)} fusion(f32[4,6,16,64,128]{4,3,2,1,0:T(8,128)} %fusion.3, f32[4,16,128]{2,1,0:T(8,128)S(1)} %copy-done.7, f32[4,16,64]{2,1,0:T(8,128)S(1)} %copy-done.9, f32[4,16]{1,0:T(4,128)S(1)} %bitcast.139, f32[4,16,128]{2,1,0:T(8,128)S(1)} %get-tuple-element.62, f32[4,16,64]{2,1,0:T(8,128)S(1)} %copy-done.5, ...), kind=kLoop, calls=%fused_computation.4 | loop fusion | flops 7864320 | bytes 4441344 | tf_op jit(solution)/shard_map/stack | solution.py:154
  (96 shorter events, 1.5 us)
Async XLA Ops:
  7.2 2.7 %copy-start = (bf16[512,1024]{1,0:T(8,128)(2,1)S(1)}, bf16[512,1024]{1,0:T(8,128)(2,1)}, u32[]{:S(2)}) copy-start(bf16[512,1024]{1,0:T(8,128)(2,1)} %param.23) | copy-start | bytes 3145732
  7.2 4.0 %copy-start.1 = (bf16[160,512]{1,0:T(8,128)(2,1)S(1)}, bf16[160,512]{1,0:T(8,128)(2,1)}, u32[]{:S(2)}) copy-start(bf16[160,512]{1,0:T(8,128)(2,1)} %param.21) | copy-start | bytes 491524
  7.2 4.0 %copy-start.14 = (f32[512]{0:T(512)S(1)}, f32[512]{0:T(512)}, u32[]{:S(2)}) copy-start(f32[512]{0:T(512)} %param.22) | copy-start | bytes 6148
  7.2 4.0 %copy-start.2 = (bf16[512,1024]{1,0:T(8,128)(2,1)S(1)}, bf16[512,1024]{1,0:T(8,128)(2,1)}, u32[]{:S(2)}) copy-start(bf16[512,1024]{1,0:T(8,128)(2,1)} %param.24) | copy-start | bytes 3145732
  7.2 158.5 %reduce-scatter.5.cloned.1.call-start = ((), (), s32[]{:S(2)}) async-start(), calls=%async_computation.1 | async-start | bytes 204800 | tf_op jit(solution)/shard_map/reduce_scatter | solution.py:151
  11.2 35.4 %copy-start.27 = (s32[4]{0:T(128)S(1)}, s32[4]{0:T(128)}, u32[]{:S(2)}) copy-start(s32[4]{0:T(128)} %param.41) | copy-start | bytes 52
  11.2 35.5 %copy-start.30 = (f32[16]{0:T(128)S(1)}, f32[16]{0:T(128)}, u32[]{:S(2)}) copy-start(f32[16]{0:T(128)} %param.32) | copy-start | bytes 196
  11.2 35.5 %copy-start.22 = (f32[4,256]{1,0:T(4,128)S(1)}, f32[4,256]{1,0:T(4,128)}, u32[]{:S(2)}) copy-start(f32[4,256]{1,0:T(4,128)} %param.29) | copy-start | bytes 12292
  11.3 36.1 %copy-start.25 = (u32[32]{0:T(128)S(1)}, u32[32]{0:T(128)}, u32[]{:S(2)}) copy-start(u32[32]{0:T(128)} %constant.48) | copy-start | bytes 388
  11.3 59.0 %copy-start.28 = (bf16[4,8,256]{2,1,0:T(8,128)(2,1)S(1)}, bf16[4,8,256]{2,1,0:T(8,128)(2,1)}, u32[]{:S(2)}) copy-start(bf16[4,8,256]{2,1,0:T(8,128)(2,1)} %param.40) | copy-start | bytes 49156
  11.3 59.8 %copy-start.29 = (bf16[4,8,256]{2,1,0:T(8,128)(2,1)S(1)}, bf16[4,8,256]{2,1,0:T(8,128)(2,1)}, u32[]{:S(2)}) copy-start(bf16[4,8,256]{2,1,0:T(8,128)(2,1)} %param.39) | copy-start | bytes 49156
  11.3 60.6 %copy-start.21 = (f32[20,16]{0,1:T(8,128)S(1)}, f32[20,16]{0,1:T(8,128)}, u32[]{:S(2)}) copy-start(f32[20,16]{0,1:T(8,128)} %param.34) | copy-start | bytes 3844
  11.3 60.7 %copy-start.19 = (f32[4,1024]{1,0:T(4,128)S(1)}, f32[4,1024]{1,0:T(4,128)}, u32[]{:S(2)}) copy-start(f32[4,1024]{1,0:T(4,128)} %param.28) | copy-start | bytes 49156
  11.3 61.3 %copy-start.12 = (bf16[4,8,1024]{2,1,0:T(8,128)(2,1)S(1)}, bf16[4,8,1024]{2,1,0:T(8,128)(2,1)}, u32[]{:S(2)}) copy-start(bf16[4,8,1024]{2,1,0:T(8,128)(2,1)} %param.38) | copy-start | bytes 196612
  43.2 40.8 %collective-permute-start = (bf16[24,2560]{1,0:T(8,128)(2,1)S(1)}, bf16[24,2560]{1,0:T(8,128)(2,1)}, u32[]{:S(2)}, u32[]{:S(2)}) collective-permute-start(bf16[24,2560]{1,0:T(8,128)(2,1)S(1)} %fusion), channel_id=1, source_target_pairs={{0,4},{4,8},{8,12},{12,16},{16,20},{20,24},{24,28},{1,5},{5,9},{9,... | collective-permute-start | bytes 368648
  45.2 38.2 %collective-permute-start.1 = (bf16[4,2560]{1,0:T(4,128)(2,1)S(1)}, bf16[4,2560]{1,0:T(4,128)(2,1)S(1)}, u32[]{:S(2)}, u32[]{:S(2)}) collective-permute-start(bf16[4,2560]{1,0:T(4,128)(2,1)S(1)} %slice.252), channel_id=1, source_target_pairs={{0,8},{4,12},{8,16},{12,20},{16,24},{20,28},{1,9},{5,13},{9,17},{1... | collective-permute-start | bytes 61448
  70.1 1.0 copy-start.24
  80.0 1.5 copy-start.26
  80.0 2.1 %copy-start.23 = (f32[4,256]{1,0:T(4,128)S(1)}, f32[4,256]{1,0:T(4,128)}, u32[]{:S(2)}) copy-start(f32[4,256]{1,0:T(4,128)} %param.30) | copy-start | bytes 12292
  83.4 0.6 copy-start.16
  86.0 8.2 %copy-start.10 = (f32[4,1,16]{2,1,0:T(1,128)S(1)}, f32[4,1,16]{2,1,0:T(1,128)}, u32[]{:S(2)}) copy-start(f32[4,1,16]{2,1,0:T(1,128)} %get-tuple-element.35) | copy-start | bytes 772
  86.0 8.2 %copy-start.11 = (f32[4,1,16]{2,1,0:T(1,128)S(1)}, f32[4,1,16]{2,1,0:T(1,128)}, u32[]{:S(2)}) copy-start(f32[4,1,16]{2,1,0:T(1,128)} %get-tuple-element.34) | copy-start | bytes 772
  86.7 0.7 copy-start.3
  93.1 4.8 %copy-start.13 = (f32[4,1,16]{2,1,0:T(1,128)S(1)}, f32[4,1,16]{2,1,0:T(1,128)}, u32[]{:S(2)}) copy-start(f32[4,1,16]{2,1,0:T(1,128)} %get-tuple-element.31) | copy-start | bytes 772
  93.1 4.8 %copy-start.15 = (f32[4,1,16]{2,1,0:T(1,128)S(1)}, f32[4,1,16]{2,1,0:T(1,128)}, u32[]{:S(2)}) copy-start(f32[4,1,16]{2,1,0:T(1,128)} %get-tuple-element.33) | copy-start | bytes 772
  93.2 4.6 %copy-start.20 = (f32[16]{0:T(128)S(1)}, f32[16]{0:T(128)}, u32[]{:S(2)}) copy-start(f32[16]{0:T(128)} %param.33) | copy-start | bytes 196
  93.2 4.6 %copy-start.17 = (f32[4,1,16]{2,1,0:T(1,128)S(1)}, f32[4,1,16]{2,1,0:T(1,128)}, u32[]{:S(2)}) copy-start(f32[4,1,16]{2,1,0:T(1,128)} %get-tuple-element.32) | copy-start | bytes 772
  93.3 10.3 %copy-start.6 = (f32[4,16,128]{2,1,0:T(8,128)}, f32[4,16,128]{2,1,0:T(8,128)S(1)}, u32[]{:S(2)}) copy-start(f32[4,16,128]{2,1,0:T(8,128)S(1)} %get-tuple-element.63) | copy-start | bytes 98308
  94.2 9.5 %copy-start.4 = (f32[4,16,64]{2,1,0:T(8,128)}, f32[4,16,64]{2,1,0:T(8,128)S(1)}, u32[]{:S(2)}) copy-start(f32[4,16,64]{2,1,0:T(8,128)S(1)} %get-tuple-element.21) | copy-start | bytes 49156
  94.2 9.5 %copy-start.8 = (f32[4,16,64]{2,1,0:T(8,128)}, f32[4,16,64]{2,1,0:T(8,128)S(1)}, u32[]{:S(2)}) copy-start(f32[4,16,64]{2,1,0:T(8,128)S(1)} %get-tuple-element.20) | copy-start | bytes 49156
  152.4 3.3 %copy-start.5 = (f32[4,16,64]{2,1,0:T(8,128)S(1)}, f32[4,16,64]{2,1,0:T(8,128)}, u32[]{:S(2)}) copy-start(f32[4,16,64]{2,1,0:T(8,128)} %copy-done.4) | copy-start | bytes 49156
  155.7 4.8 %copy-start.7 = (f32[4,16,128]{2,1,0:T(8,128)S(1)}, f32[4,16,128]{2,1,0:T(8,128)}, u32[]{:S(2)}) copy-start(f32[4,16,128]{2,1,0:T(8,128)} %copy-done.6) | copy-start | bytes 98308
  155.7 4.8 %copy-start.9 = (f32[4,16,64]{2,1,0:T(8,128)S(1)}, f32[4,16,64]{2,1,0:T(8,128)}, u32[]{:S(2)}) copy-start(f32[4,16,64]{2,1,0:T(8,128)} %copy-done.8) | copy-start | bytes 49156
  155.7 4.8 %copy-start.18 = (f32[4,1,16]{2,1,0:T(1,128)S(1)}, f32[4,1,16]{2,1,0:T(1,128)}, u32[]{:S(2)}) copy-start(f32[4,1,16]{2,1,0:T(1,128)} %get-tuple-element.32) | copy-start | bytes 772
Sparse Core Ops, SparseCore 0:
  148.0 17.0 reduce-scatter.4
where the time goes:
time: 174 us; the launch traced here: 173 us
  blocking collectives  84.9 us (49%)
  other arithmetic  44.9 us (26%)
  between operations  15.9 us (9%)
  local copies, waits for them, and re-layouts  13.6 us (8%)
  matrix products  9.89 us (6%)
  starting transfers between devices  3.28 us (2%)
    unnamed x2, blocking collectives  52 us
    all_gather x1, blocking collectives, per_device(): lax.all_gather(normed, 'kv', axis=0, tiled=True)  33 us
    unnamed x9, other arithmetic  14.5 us
    reduce_sum x2, other arithmetic, per_device(): jnp.sum(carried * conv_read[:, position][:, :, None, :], axis=-1)  8.63 us
    unnamed x70, local copies, waits for them, and re-layouts  7.38 us
    reduce_sum x1, other arithmetic, per_device(): jnp.sum(jnp.where(chosen[:, :, None, None, None], cached_state_history, 0...  6.54 us
    another operation x1, other arithmetic, per_device(): next_states = jnp.stack(states, axis=1)  5.23 us
    dot_general x4, matrix products, per_device(): jnp.dot(scaled, weight, preferred_element_type=jnp.float32)  4.25 us
  transfers between devices with their start and end apart: 3, of which 0 were waited for; matrix products, arithmetic and copies ran while one was open for 19% of the time, Pallas kernels for 0%

commit v1 on v0

v1 whole, which is shorter than its diff:
```python
import functools

import jax
import jax.numpy as jnp
from jax import lax
from jax.experimental import pallas as pl
from jax.experimental.pallas import tpu as pltpu
from jax.sharding import PartitionSpec as P

P_SIZE = 64
N = 128
TAPS = 4
DRAFT_TOKENS = 5
MESH = pl.DeviceIdType.MESH
HIGH = lax.Precision.HIGHEST
f32, bf16 = jnp.float32, jnp.bfloat16
epsilon = 1e-05


def factor(count):
    low = max(d for d in range(1, count + 1) if count % d == 0 and d * d <= count)
    return count // low, low


def remote(src, dst, send, recv, where):
    return pltpu.make_async_remote_copy(
        src_ref=src, dst_ref=dst, send_sem=send, recv_sem=recv, device_id=where, device_id_type=MESH
    )


def greet(places):
    barrier = pltpu.get_barrier_semaphore()
    for place in places:
        pl.semaphore_signal(barrier, inc=1, device_id=place, device_id_type=MESH)
    pl.semaphore_wait(barrier, len(places))


def project_kernel(
    nz, ny, own, model_width,
    tokens, gain, w_in, w_gate, w_write, w_read, step_matrix, bias, decay, extra,
    fresh_in, fresh_gate, fresh_write, fresh_read, steps_out, logs_out,
    wide, ordered, step_block, tot, *rest,
):
    pieces = 3
    send_y, recv_y, send_a, send_b, recv_a, recv_b = [
        rest[i * pieces : (i + 1) * pieces] for i in range(6)
    ]
    step_sem, sy, ry, sza, rza, szb, rzb = rest[6 * pieces :]
    me = lax.axis_index("kv")
    col = lax.axis_index("tp")
    z, y = me // ny, lax.rem(me, ny)
    width = tokens.shape[1]
    heads = bias.shape[1]
    head_rows = own - own % 16
    step_copy = pltpu.make_async_copy(
        step_matrix.at[pl.ds(pl.multiple_of(me * width, 128), width)], step_block, step_sem
    )
    step_copy.start()
    y_peers = [z * ny + lax.rem(y + d, ny) for d in range(1, ny)]
    z_peers = [lax.rem(z + d, nz) * ny + y for d in range(1, nz)]
    barrier = pltpu.get_barrier_semaphore()
    for peer in y_peers + z_peers:
        pl.semaphore_signal(barrier, inc=1, device_id={"kv": peer}, device_id_type=MESH)

    wide[...] = tokens[...].astype(f32)
    for yy in range(ny):
        for zz in range(nz):
            at = (yy * nz + zz) * own
            source = (zz * ny + yy) * own
            ordered[at : at + own] = wide[source : source + own]
    values = ordered[...]
    squares = jnp.sum(values * values, axis=1, keepdims=True)
    scaled = (values * gain[...]).astype(bf16)
    block = nz * own
    step_copy.wait()
    pick = (
        lax.broadcasted_iota(jnp.int32, (step_block.shape[1], 128), 0)
        == lax.broadcasted_iota(jnp.int32, (step_block.shape[1], 128), 1) + col * heads
    ) & (lax.broadcasted_iota(jnp.int32, (step_block.shape[1], 128), 1) < heads)
    picked = jnp.dot(
        step_block[...], pick.astype(f32).astype(bf16), preferred_element_type=f32
    ).astype(bf16)
    lane = lax.broadcasted_iota(jnp.int32, (block, 128), 1)
    sw = w_write.shape[1]

    def start_y(piece):
        copies = []
        for d in range(1, ny):
            copy = remote(
                send_y[piece].at[lax.rem(y + d, ny)], recv_y[piece].at[d - 1],
                sy.at[piece, d - 1], ry.at[piece, d - 1], {"kv": y_peers[d - 1]},
            )
            copy.start()
            copies.append(copy)
        return copies

    y_copies = []
    for piece in range(pieces):
        for yy in range(ny):
            rows = scaled[yy * block : (yy + 1) * block]
            if piece == 0:
                send_y[0][yy, :, :sw] = jnp.dot(rows, w_write[...], preferred_element_type=f32).astype(bf16)
                send_y[0][yy, :, sw : 2 * sw] = jnp.dot(rows, w_read[...], preferred_element_type=f32).astype(bf16)
                term = jnp.dot(rows, picked, preferred_element_type=f32)
                term = jnp.where(lane == heads, squares[yy * block : (yy + 1) * block], term)
                send_y[0][yy, :, 2 * sw :] = term.astype(bf16)
            else:
                weight = w_in if piece == 1 else w_gate
                send_y[piece][yy] = jnp.dot(rows, weight[...], preferred_element_type=f32).astype(bf16)
        if piece == 0:
            pl.semaphore_wait(barrier, len(y_peers) + len(z_peers))
        y_copies.append(start_y(piece))

    z_copies = []
    for piece in range(pieces):
        for copy in y_copies[piece]:
            copy.wait_recv()
        total = send_y[piece][y].astype(f32)
        for d in range(1, ny):
            total = total + recv_y[piece][d - 1].astype(f32)
        cw = total.shape[1]
        tot[:, :cw] = total
        for zz in range(nz):
            at = zz * own
            send_a[piece][zz] = tot[at : at + head_rows, :cw].astype(bf16)
            send_b[piece][zz] = tot[at + head_rows : at + own, :cw].astype(bf16)
        copies = []
        for d in range(1, nz):
            to = lax.rem(z + d, nz)
            for buf, landing, ss, rs in (
                (send_a, recv_a, sza, rza), (send_b, recv_b, szb, rzb)
            ):
                copy = remote(
                    buf[piece].at[to], landing[piece].at[d - 1],
                    ss.at[piece, d - 1], rs.at[piece, d - 1], {"kv": z_peers[d - 1]},
                )
                copy.start()
                copies.append(copy)
        z_copies.append(copies)

    inverse = None
    seqs = own // DRAFT_TOKENS
    lead = TAPS - 1
    for piece in range(pieces):
        for copy in z_copies[piece]:
            copy.wait_recv()
        total_a = send_a[piece][z].astype(f32)
        total_b = send_b[piece][z].astype(f32)
        for d in range(1, nz):
            total_a = total_a + recv_a[piece][d - 1].astype(f32)
            total_b = total_b + recv_b[piece][d - 1].astype(f32)
        cw = total_a.shape[1]
        tot[:head_rows, :cw] = total_a
        tot[head_rows:own, :cw] = total_b
        full = tot[:own, :cw]
        if piece == 0:
            tailing = full[:, 2 * sw :]
            inverse = lax.rsqrt(tailing[:, heads : heads + 1] / model_width + epsilon)
            raw = tailing[:, :heads] * inverse
            steps = jax.nn.softplus(raw + bias[...])
            logs = -steps * jnp.exp(decay[...]) + extra[...]
            fresh = (full[:, : 2 * sw] * inverse).astype(bf16).astype(f32)
            steps_out[...] = jnp.zeros_like(steps_out)
            logs_out[...] = jnp.zeros_like(logs_out)
            fresh_write[...] = jnp.zeros_like(fresh_write)
            fresh_read[...] = jnp.zeros_like(fresh_read)
            for s in range(seqs):
                cut = slice(s * DRAFT_TOKENS, (s + 1) * DRAFT_TOKENS)
                steps_out[s, :DRAFT_TOKENS] = steps[cut]
                logs_out[s, :DRAFT_TOKENS] = logs[cut]
                fresh_write[s, lead : lead + DRAFT_TOKENS] = fresh[cut, :sw]
                fresh_read[s, lead : lead + DRAFT_TOKENS] = fresh[cut, sw:]
        else:
            fresh = (full * inverse).astype(bf16).astype(f32)
            target = fresh_in if piece == 1 else fresh_gate
            first = lead if piece == 1 else 0
            target[...] = jnp.zeros_like(target)
            for s in range(seqs):
                cut = slice(s * DRAFT_TOKENS, (s + 1) * DRAFT_TOKENS)
                target[s, first : first + DRAFT_TOKENS] = fresh[cut]
    for copies in y_copies + z_copies:
        for copy in copies:
            copy.wait_send()


def state_kernel(
    group_width,
    accepted,
    fresh_in, fresh_gate, fresh_write, fresh_read, steps, logs,
    in_kernel, write_kernel, read_kernel, bypass, gain,
    saved_in, saved_write, saved_read, history,
    states, next_in, next_write, next_read, normed,
):
    taken = accepted[pl.program_id(0)]
    rows = DRAFT_TOKENS + TAPS - 1
    heads = steps.shape[2]
    width = in_kernel.shape[1]
    picks = (
        (lax.broadcasted_iota(jnp.int32, (rows, rows), 1)
         == lax.broadcasted_iota(jnp.int32, (rows, rows), 0) + taken)
        & (lax.broadcasted_iota(jnp.int32, (rows, rows), 0) < TAPS - 1)
    ).astype(f32).astype(bf16)

    def convolve(saved, fresh, taps, out):
        window = jnp.dot(picks, saved[0], preferred_element_type=f32) + fresh[0]
        out[0] = window.astype(bf16)
        total = taps[0:1] * window
        for k in range(1, TAPS):
            total = total + taps[k : k + 1] * pltpu.roll(window, rows - k, 0)
        return jax.nn.silu(total)

    x = convolve(saved_in, fresh_in, in_kernel, next_in)
    w = convolve(saved_write, fresh_write, write_kernel, next_write)
    r = convolve(saved_read, fresh_read, read_kernel, next_read)
    row = lax.broadcasted_iota(jnp.int32, (rows, heads), 0)
    log = logs[0]
    decay = jnp.zeros_like(log)
    for t in range(DRAFT_TOKENS):
        decay = decay + jnp.where(row >= t, log[t : t + 1], 0.0)
    keep = jnp.exp(decay)
    spread = (
        lax.broadcasted_iota(jnp.int32, (heads, width), 0)
        == lax.broadcasted_iota(jnp.int32, (heads, width), 1) // P_SIZE
    ).astype(f32)
    expand = functools.partial(jnp.dot, precision=HIGH, preferred_element_type=f32)
    decay_e = expand(decay, spread)
    step_x = expand(steps[0], spread) * x
    wide_row = lax.broadcasted_iota(jnp.int32, (rows, width), 0)
    direct = expand(jnp.broadcast_to(bypass[...], (rows, heads)), spread) * x
    groups = width // group_width
    per_group = group_width // P_SIZE
    gate = fresh_gate[0]
    gate = gate * jax.nn.sigmoid(gate)
    for g in range(groups):
        cut = slice(g * group_width, (g + 1) * group_width)
        wg, rg = w[:, g * N : (g + 1) * N], r[:, g * N : (g + 1) * N]
        hs = slice(g * per_group, (g + 1) * per_group)
        start = history[0, 0, hs].reshape(group_width, N)
        y = lax.dot_general(
            rg.astype(bf16), start.astype(bf16), (((1,), (1,)), ((), ())),
            preferred_element_type=f32,
        )
        dg, sg, mask_row = decay_e[:, cut], step_x[:, cut], wide_row[:, cut]
        y = y * jnp.exp(dg) + direct[:, cut]
        overlap = lax.dot_general(
            rg, wg, (((1,), (1,)), ((), ())), precision=HIGH, preferred_element_type=f32
        )
        for j in range(DRAFT_TOKENS):
            live = mask_row >= j
            fade = jnp.exp(jnp.where(live, dg - dg[j : j + 1], 0.0))
            y = y + jnp.where(live, fade * overlap[:, j : j + 1] * sg[j : j + 1], 0.0)
        gated = y * gate[:, cut]
        gated = gated * lax.rsqrt(jnp.mean(gated * gated, axis=1, keepdims=True) + epsilon)
        normed[0, :, cut] = gated * gain[:, cut]
        terms = []
        sides = []
        wide_w = jnp.concatenate([wg] * DRAFT_TOKENS, axis=1)
        lane = lax.broadcasted_iota(jnp.int32, wide_w.shape, 1) // N
        for t in range(DRAFT_TOKENS):
            live = mask_row <= t
            fade = jnp.exp(jnp.where(live, dg[t : t + 1] - dg, 0.0))
            terms.append(jnp.where(live, fade * sg, 0.0))
            sides.append(jnp.where(lane == t, wide_w, 0.0))
        left = jnp.concatenate(terms, axis=0).T.astype(bf16)
        added = jnp.dot(
            left, jnp.concatenate(sides, axis=0).astype(bf16), preferred_element_type=f32
        )
        for i in range(per_group):
            h = g * per_group + i
            own = history[0, 0, h]
            states[0, 0, h] = own
            for t in range(DRAFT_TOKENS):
                factor_th = jnp.broadcast_to(keep[t : t + 1, h : h + 1], (P_SIZE, N))
                states[0, t + 1, h] = (
                    factor_th * own
                    + added[i * P_SIZE : (i + 1) * P_SIZE, t * N : (t + 1) * N]
                )


def output_kernel(
    nz, ny, nt, own,
    normed, matrix, out,
    weight, rows_own, all_a, all_b, rows_b, send_a, send_b, recv_a, recv_b, final,
    w_sem, sz, rz, sy, ry, st, rt,
):
    me = lax.axis_index("kv")
    col = lax.axis_index("tp")
    z, y = me // ny, lax.rem(me, ny)
    w_copy = pltpu.make_async_copy(matrix, weight, w_sem)
    w_copy.start()
    head_rows = own - own % 16
    tail_rows = own - head_rows
    y_peers = [{"kv": z * ny + lax.rem(y + d, ny)} for d in range(1, ny)]
    z_peers = [{"kv": lax.rem(z + d, nz) * ny + y} for d in range(1, nz)]
    t_peers = [{"tp": lax.rem(col + d, nt)} for d in range(1, nt)]
    for s in range(own // DRAFT_TOKENS):
        rows_own[s * DRAFT_TOKENS : (s + 1) * DRAFT_TOKENS] = normed[s, :DRAFT_TOKENS]
    all_a[me] = rows_own[:head_rows].astype(bf16)
    all_b[me] = rows_own[head_rows:own].astype(bf16)
    greet(y_peers + z_peers + t_peers)

    def push(chunk, sends, recvs, place):
        pair = [
            remote(buf.at[chunk], buf.at[chunk], sends.at[i], recvs.at[i], place)
            for i, buf in enumerate((all_a, all_b))
        ]
        for copy in pair:
            copy.start()
        return pair

    z_copies = [push(me, sz.at[d], rz.at[d], z_peers[d]) for d in range(nz - 1)]
    y_sent = [push(me, sy.at[0, d], ry.at[0, d], y_peers[d]) for d in range(ny - 1)]
    for d in range(1, nz):
        for copy in z_copies[d - 1]:
            copy.wait_recv()
        chunk = lax.rem(z - d + nz, nz) * ny + y
        y_sent += [push(chunk, sy.at[d, e], ry.at[d, e], y_peers[e]) for e in range(ny - 1)]
    w_copy.wait()
    for pair in y_sent:
        for copy in pair:
            copy.wait_recv()
    for k in range(nz * ny):
        rows_b[k * tail_rows : (k + 1) * tail_rows] = all_b[k].astype(f32)
    left_a = all_a[...].reshape(nz * ny * head_rows, all_a.shape[2])
    part_a = jnp.dot(left_a, weight[...], preferred_element_type=f32)
    part_b = jnp.dot(rows_b[...].astype(bf16), weight[...], preferred_element_type=f32)
    each = nz * ny // nt
    for t in range(nt):
        send_a[t] = part_a[t * each * head_rows : (t + 1) * each * head_rows].astype(bf16)
        send_b[t] = part_b[t * each * tail_rows : (t + 1) * each * tail_rows].astype(bf16)
    t_copies = []
    for d in range(1, nt):
        to = lax.rem(col + d, nt)
        for i, (buf, landing) in enumerate(((send_a, recv_a), (send_b, recv_b))):
            copy = remote(
                buf.at[to], landing.at[d - 1], st.at[d - 1, i], rt.at[d - 1, i], t_peers[d - 1]
            )
            copy.start()
            t_copies.append(copy)
    total_a = send_a[col].astype(f32)
    total_b = send_b[col].astype(f32)
    for copy in t_copies:
        copy.wait_recv()
    for d in range(1, nt):
        total_a = total_a + recv_a[d - 1].astype(f32)
        total_b = total_b + recv_b[d - 1].astype(f32)
    for k in range(each):
        final[k * own : k * own + head_rows] = total_a[k * head_rows : (k + 1) * head_rows]
        final[k * own + head_rows : (k + 1) * own] = total_b[k * tail_rows : (k + 1) * tail_rows]
    out[...] = final[...].astype(bf16)
    for pair in z_copies + y_sent:
        for copy in pair:
            copy.wait_send()
    for copy in t_copies:
        copy.wait_send()


def per_device(
    tokens, input_norm_gain, input_matrix, gate_matrix, write_matrix, read_matrix, step_matrix,
    input_kernel, write_kernel, read_kernel, step_size_bias, head_decay_logs, bypass_scale,
    extra_decay_logs, output_norm_gain, output_matrix, cached_state_history,
    cached_input_rows, cached_write_rows, cached_read_rows, accepted,
):
    kv = lax.axis_size("kv")
    nt = lax.axis_size("tp")
    nz, ny = factor(kv)
    own = tokens.shape[0] // kv
    head_rows = own - own % 16
    tail_rows = own - head_rows
    seqs = own // DRAFT_TOKENS
    rows = DRAFT_TOKENS + TAPS - 1
    local = tokens.shape[1]
    heads = step_size_bias.shape[0]
    width = input_matrix.shape[1]
    sw = write_matrix.shape[1]
    vmem = pl.BlockSpec(memory_space=pltpu.VMEM)
    hbm = pl.BlockSpec(memory_space=pl.ANY)
    sizes = (2 * sw + 128, width, width)
    dma = pltpu.SemaphoreType.DMA
    peers = max(ny - 1, 1)
    shape = jax.ShapeDtypeStruct
    fresh_in, fresh_gate, fresh_write, fresh_read, steps, logs = pl.pallas_call(
        functools.partial(project_kernel, nz, ny, own, local * kv),
        out_shape=(
            shape((seqs, rows, width), f32), shape((seqs, rows, width), f32),
            shape((seqs, rows, sw), f32), shape((seqs, rows, sw), f32),
            shape((seqs, rows, heads), f32), shape((seqs, rows, heads), f32),
        ),
        in_specs=[vmem] * 6 + [hbm] + [vmem] * 3,
        out_specs=[vmem] * 6,
        scratch_shapes=[
            pltpu.VMEM((tokens.shape[0], local), f32),
            pltpu.VMEM((tokens.shape[0], local), f32),
            pltpu.VMEM((local, step_matrix.shape[1]), bf16),
            pltpu.VMEM((nz * own, max(sizes)), f32),
        ]
        + [pltpu.VMEM((ny, nz * own, c), bf16) for c in sizes]
        + [pltpu.VMEM((peers, nz * own, c), bf16) for c in sizes]
        + [pltpu.VMEM((nz, head_rows, c), bf16) for c in sizes]
        + [pltpu.VMEM((nz, tail_rows, c), bf16) for c in sizes]
        + [pltpu.VMEM((nz - 1, head_rows, c), bf16) for c in sizes]
        + [pltpu.VMEM((nz - 1, tail_rows, c), bf16) for c in sizes]
        + [dma(())]
        + [dma((3, peers))] * 2
        + [dma((3, nz - 1))] * 4,
        compiler_params=pltpu.CompilerParams(
            collective_id=0, has_side_effects=True, vmem_limit_bytes=40 * 2**20
        ),
    )(
        tokens, input_norm_gain[None], input_matrix, gate_matrix, write_matrix, read_matrix,
        step_matrix, step_size_bias[None], head_decay_logs[None], extra_decay_logs,
    )

    def per_seq(*dims):
        return pl.BlockSpec((1,) + dims, lambda s, acc: (s,) + (0,) * len(dims))

    def same(*dims):
        return pl.BlockSpec(dims, lambda s, acc: (0,) * len(dims))

    group_width = width // (sw // N)
    next_states, next_input, next_write, next_read, normed = pl.pallas_call(
        functools.partial(state_kernel, group_width),
        grid_spec=pltpu.PrefetchScalarGridSpec(
            num_scalar_prefetch=1,
            grid=(seqs,),
            in_specs=[
                per_seq(rows, width), per_seq(rows, width), per_seq(rows, sw), per_seq(rows, sw),
                per_seq(rows, heads), per_seq(rows, heads),
                same(TAPS, width), same(TAPS, sw), same(TAPS, sw), same(1, heads), same(1, width),
                per_seq(rows, width), per_seq(rows, sw), per_seq(rows, sw),
                pl.BlockSpec((1, 1, heads, P_SIZE, N), lambda s, acc: (s, acc[s], 0, 0, 0)),
            ],
            out_specs=[
                per_seq(DRAFT_TOKENS + 1, heads, P_SIZE, N),
                per_seq(rows, width), per_seq(rows, sw), per_seq(rows, sw), per_seq(rows, width),
            ],
        ),
        out_shape=(
            shape(cached_state_history.shape, f32),
            shape(cached_input_rows.shape, bf16),
            shape(cached_write_rows.shape, bf16),
            shape(cached_read_rows.shape, bf16),
            shape((seqs, rows, width), f32),
        ),
        compiler_params=pltpu.CompilerParams(vmem_limit_bytes=40 * 2**20),
    )(
        accepted, fresh_in, fresh_gate, fresh_write, fresh_read, steps, logs,
        input_kernel, write_kernel, read_kernel, bypass_scale[None], output_norm_gain[None],
        cached_input_rows, cached_write_rows, cached_read_rows, cached_state_history,
    )

    out_width = output_matrix.shape[1]
    each = kv // nt
    mixer_out = pl.pallas_call(
        functools.partial(output_kernel, nz, ny, nt, own),
        out_shape=shape((each * own, out_width), bf16),
        in_specs=[vmem, hbm],
        out_specs=vmem,
        scratch_shapes=[
            pltpu.VMEM(output_matrix.shape, bf16),
            pltpu.VMEM((own, width), f32),
            pltpu.VMEM((kv, head_rows, width), bf16),
            pltpu.VMEM((kv, tail_rows, width), bf16),
            pltpu.VMEM((kv * tail_rows, width), f32),
            pltpu.VMEM((nt, each * head_rows, out_width), bf16),
            pltpu.VMEM((nt, each * tail_rows, out_width), bf16),
            pltpu.VMEM((nt - 1, each * head_rows, out_width), bf16),
            pltpu.VMEM((nt - 1, each * tail_rows, out_width), bf16),
            pltpu.VMEM((each * own, out_width), f32),
            dma(()),
            dma((nz - 1, 2)), dma((nz - 1, 2)),
            dma((nz, peers, 2)), dma((nz, peers, 2)),
            dma((nt - 1, 2)), dma((nt - 1, 2)),
        ],
        compiler_params=pltpu.CompilerParams(
            collective_id=1, has_side_effects=True, vmem_limit_bytes=40 * 2**20
        ),
    )(normed, output_matrix)
    return mixer_out, next_states, next_input, next_write, next_read


def solution(mesh):
    return jax.shard_map(
        per_device,
        mesh=mesh,
        in_specs=(
            P(None, "kv"),
            P("kv"),
            P("kv", "tp"),
            P("kv", "tp"),
            P("kv", "tp"),
            P("kv", "tp"),
            P(),
            P(None, "tp"),
            P(None, "tp"),
            P(None, "tp"),
            P("tp"),
            P("tp"),
            P("tp"),
            P("kv", "tp"),
            P("tp"),
            P("tp", "kv"),
            P("kv", None, "tp", None, None),
            P("kv", None, "tp"),
            P("kv", None, "tp"),
            P("kv", None, "tp"),
            P("kv"),
        ),
        out_specs=(
            P("tp", "kv"),
            P("kv", None, "tp", None, None),
            P("kv", None, "tp"),
            P("kv", None, "tp"),
            P("kv", None, "tp"),
        ),
        check_vma=False,
    )
```

time: 174 us -> 65.2 us (0.37)
  blocking collectives: 84.9 us -> 0 us
  other arithmetic: 44.9 us -> 0 us
  Pallas kernels: 0 us -> 42.6 us
  between operations: 15.9 us -> 0.7 us
  matrix products: 9.89 us -> 0 us
  local copies, waits for them, and re-layouts: 13.6 us -> 21.2 us
  starting transfers between devices: 3.28 us -> 0 us
    unnamed x2 -> x0, blocking collectives: 52 us -> none
    pallas_call x0 -> x3, Pallas kernels: none -> 42.6 us  [the longest x1 21.5 us: per_device(): pl.pallas_call(functools.partial(project_kernel, nz, ny, own, local * kv)...]
    all_gather x1 -> x0, blocking collectives: 33 us -> none  [per_device(): lax.all_gather(normed, 'kv', axis=0, tiled=True)]
    reduce_sum x5 -> x0, other arithmetic: 16.3 us -> none  [the longest x2 8.63 us: per_device(): jnp.sum(carried * conv_read[:, position][:, :, None, :], axis=-1)]
    unnamed x9 -> x0, other arithmetic: 14.5 us -> none
    unnamed x70 -> x41, local copies, waits for them, and re-layouts: 7.38 us -> 21.2 us
    dot_general x9 -> x0, matrix products: 9.89 us -> none  [the longest x4 4.25 us: per_device(): jnp.dot(scaled, weight, preferred_element_type=jnp.float32)]
    another operation x2 -> x0, other arithmetic: 5.31 us -> none  [the longest x1 5.23 us: per_device(): next_states = jnp.stack(states, axis=1)]
  transfers between devices with their start and end apart: 3 -> 0, of which waited for: 0 -> 0; matrix products, arithmetic and copies ran while one was open for 19% -> 0% of each run, Pallas kernels for 0% -> 0%
where the time goes in v1:
time: 65.2 us; the launch traced here: 64.5 us
  Pallas kernels  42.6 us (65%)
  local copies, waits for them, and re-layouts  21.2 us (33%)
  between operations  0.7 us (1%)
    pallas_call x1, Pallas kernels, per_device(): pl.pallas_call(functools.partial(project_kernel, nz, ny, own, local * kv)...  21.5 us
    unnamed x41, local copies, waits for them, and re-layouts  21.2 us
    pallas_call x1, Pallas kernels, per_device(): pl.pallas_call(functools.partial(output_kernel, nz, ny, nt, own), out_sha...  14.2 us
    pallas_call x1, Pallas kernels, per_device(): pl.pallas_call(functools.partial(state_kernel, group_width), grid_spec=pl...  6.95 us

profile of v1, /device:TPU:0, one launch (start us, length us, event | category | flops | bytes accessed | tf_op | source)
XLA Modules:
  0.0 64.5 jit_solution(11016925079198347834)
XLA Ops:
  0.6 0.0 copy-start.3
  0.6 0.9 %copy.27.extra = f32[20,16]{1,0:T(8,128)S(1)} copy(f32[20,16]{0,1:T(8,128)} %param.34) | data formatting | bytes 2560 | tf_op args[13]
  1.5 1.5 %copy.26.step_matrix = bf16[4096,64]{1,0:T(8,128)(2,1)S(1)} copy(bf16[4096,64]{0,1:T(8,128)(2,1)} %param.27) | data formatting | bytes 1048576 | tf_op args[6]
  3.0 0.0 copy-start.1
  3.0 1.2 %copy-done.1 = bf16[512,1024]{1,0:T(8,128)(2,1)S(1)} copy-done((bf16[512,1024]{1,0:T(8,128)(2,1)S(1)}, bf16[512,1024]{1,0:T(8,128)(2,1)}, u32[]{:S(2)}) %copy-start.1) | copy-done | bytes 1048600
  4.3 0.0 copy-start.2
  4.3 1.2 %copy-done.2 = bf16[512,1024]{1,0:T(8,128)(2,1)S(1)} copy-done((bf16[512,1024]{1,0:T(8,128)(2,1)S(1)}, bf16[512,1024]{1,0:T(8,128)(2,1)}, u32[]{:S(2)}) %copy-start.2) | copy-done | bytes 1048600
  5.5 0.0 copy-start.4
  5.5 0.9 %copy-done.4 = bf16[512,256]{1,0:T(8,128)(2,1)S(1)} copy-done((bf16[512,256]{1,0:T(8,128)(2,1)S(1)}, bf16[512,256]{1,0:T(8,128)(2,1)}, u32[]{:S(2)}) %copy-start.4) | copy-done | bytes 262168
  6.4 0.0 copy-start.5
  6.4 0.9 %copy-done.5 = bf16[512,256]{1,0:T(8,128)(2,1)S(1)} copy-done((bf16[512,256]{1,0:T(8,128)(2,1)S(1)}, bf16[512,256]{1,0:T(8,128)(2,1)}, u32[]{:S(2)}) %copy-start.5) | copy-done | bytes 262168
  7.4 0.0 copy-start.6
  7.4 0.9 %copy-done.6 = bf16[160,512]{1,0:T(8,128)(2,1)S(1)} copy-done((bf16[160,512]{1,0:T(8,128)(2,1)S(1)}, bf16[160,512]{1,0:T(8,128)(2,1)}, u32[]{:S(2)}) %copy-start.6) | copy-done | bytes 163864
  8.3 0.0 copy-start.14
  8.3 0.7 %copy-done.14 = f32[512]{0:T(512)S(1)} copy-done((f32[512]{0:T(512)S(1)}, f32[512]{0:T(512)}, u32[]{:S(2)}) %copy-start.14) | copy-done | bytes 2072
  9.0 0.0 copy-start.15
  9.0 0.7 %copy-done.15 = f32[16]{0:T(128)S(1)} copy-done((f32[16]{0:T(128)S(1)}, f32[16]{0:T(128)}, u32[]{:S(2)}) %copy-start.15) | copy-done | bytes 88
  9.6 0.0 copy-start.16
  9.6 0.7 %copy-done.16 = f32[16]{0:T(128)S(1)} copy-done((f32[16]{0:T(128)S(1)}, f32[16]{0:T(128)}, u32[]{:S(2)}) %copy-start.16) | copy-done | bytes 88
  10.3 21.5 %shard_map.236 = (f32[4,8,1024]{2,1,0:T(8,128)S(1)}, f32[4,8,1024]{2,1,0:T(8,128)S(1)}, f32[4,8,256]{2,1,0:T(8,128)S(1)}, f32[4,8,256]{2,1,0:T(8,128)S(1)}, f32[...) custom-call(bf16[160,512]{1,0:T(8,128)(2,1)S(1)} %copy-done.6, f32[1,512]{1,0:T(1,128)S(1)} %bitcast.6, ...), custom_call_target="tpu_custom_call" | custom-call | tf_op jit(solution)/shard_map/pallas_call | solution.py:382
  31.8 0.0 copy-start
  31.8 4.6 %copy-done = f32[4,6,16,64,128]{4,3,2,1,0:T(8,128)S(1)} copy-done((f32[4,6,16,64,128]{4,3,2,1,0:T(8,128)S(1)}, f32[4,6,16,64,128]{4,3,2,1,0:T(8,128)}, u32[]{:S(2)}) %copy-start) | copy-done | bytes 12582936
  36.3 0.0 copy-start.7
  36.3 0.8 %copy-done.7 = bf16[4,8,1024]{2,1,0:T(8,128)(2,1)S(1)} copy-done((bf16[4,8,1024]{2,1,0:T(8,128)(2,1)S(1)}, bf16[4,8,1024]{2,1,0:T(8,128)(2,1)}, u32[]{:S(2)}) %copy-start.7) | copy-done | bytes 65560
  37.2 0.0 copy-start.8
  37.2 0.7 %copy-done.8 = f32[4,1024]{1,0:T(4,128)S(1)} copy-done((f32[4,1024]{1,0:T(4,128)S(1)}, f32[4,1024]{1,0:T(4,128)}, u32[]{:S(2)}) %copy-start.8) | copy-done | bytes 16408
  37.9 0.0 copy-start.9
  37.9 0.7 %copy-done.9 = bf16[4,8,256]{2,1,0:T(8,128)(2,1)S(1)} copy-done((bf16[4,8,256]{2,1,0:T(8,128)(2,1)S(1)}, bf16[4,8,256]{2,1,0:T(8,128)(2,1)}, u32[]{:S(2)}) %copy-start.9) | copy-done | bytes 16408
  38.6 0.0 copy-start.10
  38.6 0.7 %copy-done.10 = bf16[4,8,256]{2,1,0:T(8,128)(2,1)S(1)} copy-done((bf16[4,8,256]{2,1,0:T(8,128)(2,1)S(1)}, bf16[4,8,256]{2,1,0:T(8,128)(2,1)}, u32[]{:S(2)}) %copy-start.10) | copy-done | bytes 16408
  39.3 0.0 copy-start.11
  39.3 0.7 %copy-done.11 = f32[4,256]{1,0:T(4,128)S(1)} copy-done((f32[4,256]{1,0:T(4,128)S(1)}, f32[4,256]{1,0:T(4,128)}, u32[]{:S(2)}) %copy-start.11) | copy-done | bytes 4120
  40.0 0.0 copy-start.12
  40.0 0.7 %copy-done.12 = f32[4,256]{1,0:T(4,128)S(1)} copy-done((f32[4,256]{1,0:T(4,128)S(1)}, f32[4,256]{1,0:T(4,128)}, u32[]{:S(2)}) %copy-start.12) | copy-done | bytes 4120
  40.7 0.0 copy-start.13
  40.7 0.7 %copy-done.13 = f32[1024]{0:T(1024)S(1)} copy-done((f32[1024]{0:T(1024)S(1)}, f32[1024]{0:T(1024)}, u32[]{:S(2)}) %copy-start.13) | copy-done | bytes 4120
  41.4 0.0 copy-start.17
  41.4 0.7 %copy-done.17 = s32[4]{0:T(128)S(1)} copy-done((s32[4]{0:T(128)S(1)}, s32[4]{0:T(128)}, u32[]{:S(2)}) %copy-start.17) | copy-done | bytes 40
  42.1 0.0 copy-start.18
  42.1 0.7 %copy-done.18 = f32[16]{0:T(128)S(1)} copy-done((f32[16]{0:T(128)S(1)}, f32[16]{0:T(128)}, u32[]{:S(2)}) %copy-start.18) | copy-done | bytes 88
  42.7 6.9 %shard_map.237 = (f32[4,6,16,64,128]{4,3,2,1,0:T(8,128)}, bf16[4,8,1024]{2,1,0:T(8,128)(2,1)}, bf16[4,8,256]{2,1,0:T(8,128)(2,1)}, bf16[4,8,256]{2,1,0:T(8,128)(2,1)}, f32[4,8,1024]{2,1,0:T(8,128)S(1)}) custom-call(s32[4]{0:T(128)S(1)} %copy-done.17, f32[4,8,1024]{2,1,0:T(8,128)S(1)} %get-tuple-element.16.fresh_in, ...), custom_call_target="tpu_custom_call" | custom-call | tf_op jit(solution)/shard_map/pallas_call | solution.py:421
  49.7 0.0 copy-done.3
  49.7 14.2 %shard_map.238 = bf16[40,512]{1,0:T(8,128)(2,1)S(1)} custom-call(f32[4,8,1024]{2,1,0:T(8,128)S(1)} %get-tuple-element.22.normed, bf16[1024,512]{1,0:T(8,128)(2,1)S(1)} %copy-done.3), custom_call_target="tpu_custom_call" | custom-call | tf_op jit(solution)/shard_map/pallas_call | solution.py:454
  63.9 0.6 copy.29
Async XLA Ops:
  0.6 49.0 %copy-start.3 = (bf16[1024,512]{1,0:T(8,128)(2,1)S(1)}, bf16[1024,512]{1,0:T(8,128)(2,1)}, u32[]{:S(2)}) copy-start(bf16[1024,512]{1,0:T(8,128)(2,1)} %matrix.1) | copy-start | bytes 3145732
  3.0 1.2 %copy-start.1 = (bf16[512,1024]{1,0:T(8,128)(2,1)S(1)}, bf16[512,1024]{1,0:T(8,128)(2,1)}, u32[]{:S(2)}) copy-start(bf16[512,1024]{1,0:T(8,128)(2,1)} %w_in.1) | copy-start | bytes 3145732
  4.3 1.2 %copy-start.2 = (bf16[512,1024]{1,0:T(8,128)(2,1)S(1)}, bf16[512,1024]{1,0:T(8,128)(2,1)}, u32[]{:S(2)}) copy-start(bf16[512,1024]{1,0:T(8,128)(2,1)} %w_gate.1) | copy-start | bytes 3145732
  5.5 0.9 %copy-start.4 = (bf16[512,256]{1,0:T(8,128)(2,1)S(1)}, bf16[512,256]{1,0:T(8,128)(2,1)}, u32[]{:S(2)}) copy-start(bf16[512,256]{1,0:T(8,128)(2,1)} %w_write.1) | copy-start | bytes 786436
  6.4 0.9 %copy-start.5 = (bf16[512,256]{1,0:T(8,128)(2,1)S(1)}, bf16[512,256]{1,0:T(8,128)(2,1)}, u32[]{:S(2)}) copy-start(bf16[512,256]{1,0:T(8,128)(2,1)} %w_read.1) | copy-start | bytes 786436
  7.4 0.9 %copy-start.6 = (bf16[160,512]{1,0:T(8,128)(2,1)S(1)}, bf16[160,512]{1,0:T(8,128)(2,1)}, u32[]{:S(2)}) copy-start(bf16[160,512]{1,0:T(8,128)(2,1)} %tokens.1) | copy-start | bytes 491524
  8.3 0.7 %copy-start.14 = (f32[512]{0:T(512)S(1)}, f32[512]{0:T(512)}, u32[]{:S(2)}) copy-start(f32[512]{0:T(512)} %param.22) | copy-start | bytes 6148
  9.0 0.7 %copy-start.15 = (f32[16]{0:T(128)S(1)}, f32[16]{0:T(128)}, u32[]{:S(2)}) copy-start(f32[16]{0:T(128)} %param.31) | copy-start | bytes 196
  9.6 0.7 %copy-start.16 = (f32[16]{0:T(128)S(1)}, f32[16]{0:T(128)}, u32[]{:S(2)}) copy-start(f32[16]{0:T(128)} %param.32) | copy-start | bytes 196
  31.8 4.6 %copy-start = (f32[4,6,16,64,128]{4,3,2,1,0:T(8,128)S(1)}, f32[4,6,16,64,128]{4,3,2,1,0:T(8,128)}, u32[]{:S(2)}) copy-start(f32[4,6,16,64,128]{4,3,2,1,0:T(8,128)} %history.1) | copy-start | bytes 37748740
  36.3 0.8 %copy-start.7 = (bf16[4,8,1024]{2,1,0:T(8,128)(2,1)S(1)}, bf16[4,8,1024]{2,1,0:T(8,128)(2,1)}, u32[]{:S(2)}) copy-start(bf16[4,8,1024]{2,1,0:T(8,128)(2,1)} %saved_in.1) | copy-start | bytes 196612
  37.2 0.7 %copy-start.8 = (f32[4,1024]{1,0:T(4,128)S(1)}, f32[4,1024]{1,0:T(4,128)}, u32[]{:S(2)}) copy-start(f32[4,1024]{1,0:T(4,128)} %in_kernel.1) | copy-start | bytes 49156
  37.9 0.7 %copy-start.9 = (bf16[4,8,256]{2,1,0:T(8,128)(2,1)S(1)}, bf16[4,8,256]{2,1,0:T(8,128)(2,1)}, u32[]{:S(2)}) copy-start(bf16[4,8,256]{2,1,0:T(8,128)(2,1)} %saved_write.1) | copy-start | bytes 49156
  38.6 0.7 %copy-start.10 = (bf16[4,8,256]{2,1,0:T(8,128)(2,1)S(1)}, bf16[4,8,256]{2,1,0:T(8,128)(2,1)}, u32[]{:S(2)}) copy-start(bf16[4,8,256]{2,1,0:T(8,128)(2,1)} %saved_read.1) | copy-start | bytes 49156
  39.3 0.7 %copy-start.11 = (f32[4,256]{1,0:T(4,128)S(1)}, f32[4,256]{1,0:T(4,128)}, u32[]{:S(2)}) copy-start(f32[4,256]{1,0:T(4,128)} %write_kernel.1) | copy-start | bytes 12292
  40.0 0.7 %copy-start.12 = (f32[4,256]{1,0:T(4,128)S(1)}, f32[4,256]{1,0:T(4,128)}, u32[]{:S(2)}) copy-start(f32[4,256]{1,0:T(4,128)} %read_kernel.1) | copy-start | bytes 12292
  40.7 0.7 %copy-start.13 = (f32[1024]{0:T(1024)S(1)}, f32[1024]{0:T(1024)}, u32[]{:S(2)}) copy-start(f32[1024]{0:T(1024)} %param.35) | copy-start | bytes 12292
  41.4 0.7 %copy-start.17 = (s32[4]{0:T(128)S(1)}, s32[4]{0:T(128)}, u32[]{:S(2)}) copy-start(s32[4]{0:T(128)} %accepted.1) | copy-start | bytes 52
  42.1 0.7 %copy-start.18 = (f32[16]{0:T(128)S(1)}, f32[16]{0:T(128)}, u32[]{:S(2)}) copy-start(f32[16]{0:T(128)} %param.33) | copy-start | bytes 196

commit v2 on v1

--- a/solution.py
+++ b/solution.py
@@ -15,6 +15,7 @@
 HIGH = lax.Precision.HIGHEST
 f32, bf16 = jnp.float32, jnp.bfloat16
 epsilon = 1e-05
+VMEM_BYTES = 67043328
 
 
 def factor(count):
@@ -37,31 +38,42 @@
 
 def project_kernel(
     nz, ny, own, model_width,
-    tokens, gain, w_in, w_gate, w_write, w_read, step_matrix, bias, decay, extra,
+    tokens_h, gain_h, in_h, gate_h, write_h, read_h, step_h, bias_h, decay_h, extra_h,
     fresh_in, fresh_gate, fresh_write, fresh_read, steps_out, logs_out,
-    wide, ordered, step_block, tot, *rest,
+    tokens, gain, w_in, w_gate, w_write, w_read, step_block, bias, decay, extra,
+    wide, ordered, tot, load_sem, *rest,
 ):
-    pieces = 3
+    pieces = 5
     send_y, recv_y, send_a, send_b, recv_a, recv_b = [
         rest[i * pieces : (i + 1) * pieces] for i in range(6)
     ]
-    step_sem, sy, ry, sza, rza, szb, rzb = rest[6 * pieces :]
+    sy, ry, sza, rza, szb, rzb = rest[6 * pieces :]
     me = lax.axis_index("kv")
     col = lax.axis_index("tp")
     z, y = me // ny, lax.rem(me, ny)
     width = tokens.shape[1]
     heads = bias.shape[1]
     head_rows = own - own % 16
-    step_copy = pltpu.make_async_copy(
-        step_matrix.at[pl.ds(pl.multiple_of(me * width, 128), width)], step_block, step_sem
-    )
-    step_copy.start()
+    half = w_in.shape[1] // 2
+    step_cut = step_h.at[:, pl.ds(pl.multiple_of(me * width, 128), width)]
+    loads = [
+        pltpu.make_async_copy(source, target, load_sem.at[i])
+        for i, (source, target) in enumerate((
+            (tokens_h, tokens), (gain_h, gain), (step_cut, step_block), (write_h, w_write),
+            (read_h, w_read), (in_h, w_in), (gate_h, w_gate), (bias_h, bias),
+            (decay_h, decay), (extra_h, extra),
+        ))
+    ]
+    for load in loads:
+        load.start()
     y_peers = [z * ny + lax.rem(y + d, ny) for d in range(1, ny)]
     z_peers = [lax.rem(z + d, nz) * ny + y for d in range(1, nz)]
     barrier = pltpu.get_barrier_semaphore()
     for peer in y_peers + z_peers:
         pl.semaphore_signal(barrier, inc=1, device_id={"kv": peer}, device_id_type=MESH)
 
+    loads[0].wait()
+    loads[1].wait()
     wide[...] = tokens[...].astype(f32)
     for yy in range(ny):
         for zz in range(nz):
@@ -72,13 +84,14 @@
     squares = jnp.sum(values * values, axis=1, keepdims=True)
     scaled = (values * gain[...]).astype(bf16)
     block = nz * own
-    step_copy.wait()
+    for load in loads[2:5]:
+        load.wait()
+    picked_row = lax.broadcasted_iota(jnp.int32, (128, step_block.shape[0]), 0)
     pick = (
-        lax.broadcasted_iota(jnp.int32, (step_block.shape[1], 128), 0)
-        == lax.broadcasted_iota(jnp.int32, (step_block.shape[1], 128), 1) + col * heads
-    ) & (lax.broadcasted_iota(jnp.int32, (step_block.shape[1], 128), 1) < heads)
+        lax.broadcasted_iota(jnp.int32, (128, step_block.shape[0]), 1) == picked_row + col * heads
+    ) & (picked_row < heads)
     picked = jnp.dot(
-        step_block[...], pick.astype(f32).astype(bf16), preferred_element_type=f32
+        pick.astype(f32).astype(bf16), step_block[...], preferred_element_type=f32
     ).astype(bf16)
     lane = lax.broadcasted_iota(jnp.int32, (block, 128), 1)
     sw = w_write.shape[1]
@@ -96,17 +109,26 @@
 
     y_copies = []
     for piece in range(pieces):
+        if piece == 1:
+            loads[5].wait()
+        if piece == 3:
+            loads[6].wait()
         for yy in range(ny):
             rows = scaled[yy * block : (yy + 1) * block]
             if piece == 0:
                 send_y[0][yy, :, :sw] = jnp.dot(rows, w_write[...], preferred_element_type=f32).astype(bf16)
                 send_y[0][yy, :, sw : 2 * sw] = jnp.dot(rows, w_read[...], preferred_element_type=f32).astype(bf16)
-                term = jnp.dot(rows, picked, preferred_element_type=f32)
+                term = lax.dot_general(
+                    rows, picked, (((1,), (1,)), ((), ())), preferred_element_type=f32
+                )
                 term = jnp.where(lane == heads, squares[yy * block : (yy + 1) * block], term)
                 send_y[0][yy, :, 2 * sw :] = term.astype(bf16)
             else:
-                weight = w_in if piece == 1 else w_gate
-                send_y[piece][yy] = jnp.dot(rows, weight[...], preferred_element_type=f32).astype(bf16)
+                weight = w_in if piece < 3 else w_gate
+                first = (piece - 1) % 2 * half
+                send_y[piece][yy] = jnp.dot(
+                    rows, weight[:, first : first + half], preferred_element_type=f32
+                ).astype(bf16)
         if piece == 0:
             pl.semaphore_wait(barrier, len(y_peers) + len(z_peers))
         y_copies.append(start_y(piece))
@@ -138,6 +160,8 @@
                 copies.append(copy)
         z_copies.append(copies)
 
+    for load in loads[7:]:
+        load.wait()
     inverse = None
     seqs = own // DRAFT_TOKENS
     lead = TAPS - 1
@@ -158,7 +182,14 @@
             inverse = lax.rsqrt(tailing[:, heads : heads + 1] / model_width + epsilon)
             raw = tailing[:, :heads] * inverse
             steps = jax.nn.softplus(raw + bias[...])
-            logs = -steps * jnp.exp(decay[...]) + extra[...]
+            same_row = lax.broadcasted_iota(jnp.int32, (own, own), 0) == lax.broadcasted_iota(
+                jnp.int32, (own, own), 1
+            )
+            added_logs = lax.dot_general(
+                same_row.astype(f32), extra[...], (((1,), (1,)), ((), ())),
+                precision=HIGH, preferred_element_type=f32,
+            )
+            logs = -steps * jnp.exp(decay[...]) + added_logs
             fresh = (full[:, : 2 * sw] * inverse).astype(bf16).astype(f32)
             steps_out[...] = jnp.zeros_like(steps_out)
             logs_out[...] = jnp.zeros_like(logs_out)
@@ -172,12 +203,14 @@
                 fresh_read[s, lead : lead + DRAFT_TOKENS] = fresh[cut, sw:]
         else:
             fresh = (full * inverse).astype(bf16).astype(f32)
-            target = fresh_in if piece == 1 else fresh_gate
-            first = lead if piece == 1 else 0
-            target[...] = jnp.zeros_like(target)
+            target = fresh_in if piece < 3 else fresh_gate
+            first = lead if piece < 3 else 0
+            if piece % 2 == 1:
+                target[...] = jnp.zeros_like(target)
+            columns = slice((piece - 1) % 2 * half, (piece - 1) % 2 * half + half)
             for s in range(seqs):
                 cut = slice(s * DRAFT_TOKENS, (s + 1) * DRAFT_TOKENS)
-                target[s, first : first + DRAFT_TOKENS] = fresh[cut]
+                target[s, first : first + DRAFT_TOKENS, columns] = fresh[cut]
     for copies in y_copies + z_copies:
         for copy in copies:
             copy.wait_send()
@@ -375,7 +408,7 @@
     sw = write_matrix.shape[1]
     vmem = pl.BlockSpec(memory_space=pltpu.VMEM)
     hbm = pl.BlockSpec(memory_space=pl.ANY)
-    sizes = (2 * sw + 128, width, width)
+    sizes = (2 * sw + 128,) + (width // 2,) * 4
     dma = pltpu.SemaphoreType.DMA
     peers = max(ny - 1, 1)
     shape = jax.ShapeDtypeStruct
@@ -386,13 +419,23 @@
             shape((seqs, rows, sw), f32), shape((seqs, rows, sw), f32),
             shape((seqs, rows, heads), f32), shape((seqs, rows, heads), f32),
         ),
-        in_specs=[vmem] * 6 + [hbm] + [vmem] * 3,
+        in_specs=[hbm] * 10,
         out_specs=[vmem] * 6,
         scratch_shapes=[
+            pltpu.VMEM(tokens.shape, bf16),
+            pltpu.VMEM((1, local), f32),
+            pltpu.VMEM((local, width), bf16),
+            pltpu.VMEM((local, width), bf16),
+            pltpu.VMEM((local, sw), bf16),
+            pltpu.VMEM((local, sw), bf16),
+            pltpu.VMEM((step_matrix.shape[1], local), bf16),
+            pltpu.VMEM((1, heads), f32),
+            pltpu.VMEM((1, heads), f32),
+            pltpu.VMEM((heads, own), f32),
             pltpu.VMEM((tokens.shape[0], local), f32),
             pltpu.VMEM((tokens.shape[0], local), f32),
-            pltpu.VMEM((local, step_matrix.shape[1]), bf16),
             pltpu.VMEM((nz * own, max(sizes)), f32),
+            dma((10,)),
         ]
         + [pltpu.VMEM((ny, nz * own, c), bf16) for c in sizes]
         + [pltpu.VMEM((peers, nz * own, c), bf16) for c in sizes]
@@ -400,15 +443,14 @@
         + [pltpu.VMEM((nz, tail_rows, c), bf16) for c in sizes]
         + [pltpu.VMEM((nz - 1, head_rows, c), bf16) for c in sizes]
         + [pltpu.VMEM((nz - 1, tail_rows, c), bf16) for c in sizes]
-        + [dma(())]
-        + [dma((3, peers))] * 2
-        + [dma((3, nz - 1))] * 4,
+        + [dma((5, peers))] * 2
+        + [dma((5, nz - 1))] * 4,
         compiler_params=pltpu.CompilerParams(
-            collective_id=0, has_side_effects=True, vmem_limit_bytes=40 * 2**20
+            collective_id=0, has_side_effects=True, vmem_limit_bytes=VMEM_BYTES
         ),
     )(
         tokens, input_norm_gain[None], input_matrix, gate_matrix, write_matrix, read_matrix,
-        step_matrix, step_size_bias[None], head_decay_logs[None], extra_decay_logs,
+        step_matrix.T, step_size_bias[None], head_decay_logs[None], extra_decay_logs.T,
     )
 
     def per_seq(*dims):
@@ -442,7 +484,7 @@
             shape(cached_read_rows.shape, bf16),
             shape((seqs, rows, width), f32),
         ),
-        compiler_params=pltpu.CompilerParams(vmem_limit_bytes=40 * 2**20),
+        compiler_params=pltpu.CompilerParams(vmem_limit_bytes=VMEM_BYTES),
     )(
         accepted, fresh_in, fresh_gate, fresh_write, fresh_read, steps, logs,
         input_kernel, write_kernel, read_kernel, bypass_scale[None], output_norm_gain[None],
@@ -473,7 +515,7 @@
             dma((nt - 1, 2)), dma((nt - 1, 2)),
         ],
         compiler_params=pltpu.CompilerParams(
-            collective_id=1, has_side_effects=True, vmem_limit_bytes=40 * 2**20
+            collective_id=1, has_side_effects=True, vmem_limit_bytes=VMEM_BYTES
         ),
     )(normed, output_matrix)
     return mixer_out, next_states, next_input, next_write, next_read

time: 65.2 us -> 48.4 us (0.74)
  local copies, waits for them, and re-layouts: 21.2 us -> 1.4 us
  Pallas kernels: 42.6 us -> 46 us
    unnamed x41 -> x1, local copies, waits for them, and re-layouts: 21.2 us -> 1.4 us
    pallas_call x1, Pallas kernels: 6.95 us -> 9.04 us  [per_device(): pl.pallas_call(functools.partial(state_kernel, group_width), grid_spec=pl...]
    pallas_call x1, Pallas kernels: 14.2 us -> 15.5 us  [per_device(): pl.pallas_call(functools.partial(output_kernel, nz, ny, nt, own), out_sha...]
where the time goes in v2:
time: 48.4 us; the launch traced here: 48 us
  Pallas kernels  46 us (95%)
  local copies, waits for them, and re-layouts  1.4 us (3%)
  between operations  0.66 us (1%)
    pallas_call x1, Pallas kernels, per_device(): pl.pallas_call(functools.partial(project_kernel, nz, ny, own, local * kv)...  21.4 us
    pallas_call x1, Pallas kernels, per_device(): pl.pallas_call(functools.partial(output_kernel, nz, ny, nt, own), out_sha...  15.5 us
    pallas_call x1, Pallas kernels, per_device(): pl.pallas_call(functools.partial(state_kernel, group_width), grid_spec=pl...  9.04 us
    unnamed x1, local copies, waits for them, and re-layouts  1.4 us

profile of v2, /device:TPU:0, one launch (start us, length us, event | category | flops | bytes accessed | tf_op | source)
XLA Modules:
  0.0 48.0 jit_solution(2044862843303439113)
XLA Ops:
  0.6 21.4 %shard_map.236 = (f32[4,8,1024]{2,1,0:T(8,128)}, f32[4,8,1024]{2,1,0:T(8,128)}, f32[4,8,256]{2,1,0:T(8,128)}, f32[4,8,256]{2,1,0:T(8,128)}, f32[4,8,16]{2,1,0:T(8,128)}, /*index=5*/f32[4,8,16]{2,1,0:T(8,128)}) custom-call(bf16[160,512]{1,0:T(8,128)(2,1)} %tokens_h.1, f32[1,512]{1,0:T(1,128)} %bitcast.10, bf16[512,1024]{1,0:T(8,128)(2,1)} %in_h.1, ...), custom_call_target="tpu_custom_call" | custom-call | tf_op jit(solution)/shard_map/pallas_call | solution.py:415
  22.1 9.0 %shard_map.237 = (f32[4,6,16,64,128]{4,3,2,1,0:T(8,128)}, bf16[4,8,1024]{2,1,0:T(8,128)(2,1)}, bf16[4,8,256]{2,1,0:T(8,128)(2,1)}, bf16[4,8,256]{2,1,0:T(8,128)(2,1)}, f32[4,8,1024]{2,1,0:T(8,128)}) custom-call(s32[4]{0:T(128)} %accepted.1, f32[4,8,1024]{2,1,0:T(8,128)} %get-tuple-element.16.fresh_in, f32[4,8,1024]{2,1,0:T(8,128)} %get-tuple-element.17.fresh_gate, ...), custom_call_target="tpu_custom_call" | custom-call | tf_op jit(solution)/shard_map/pallas_call | solution.py:463
  31.1 15.5 %shard_map.238 = bf16[40,512]{1,0:T(8,128)(2,1)} custom-call(f32[4,8,1024]{2,1,0:T(8,128)} %get-tuple-element.22.normed, bf16[1024,512]{1,0:T(8,128)(2,1)} %matrix.1), custom_call_target="tpu_custom_call" | custom-call | tf_op jit(solution)/shard_map/pallas_call | solution.py:496
  46.6 1.4 %copy.27 = bf16[40,512]{1,0:T(8,128)(2,1)} copy(bf16[40,512]{1,0:T(8,128)(2,1)} %shard_map.238) | data formatting | bytes 81920
